TPU v7x, 32 devices: a whole 2x2x4 slice. The times are simulated.
32 devices in a mesh: rep: 4 (over z), fs: 4 (over y, x), tp: 2 (over core).
Axes of the slice: x: 2, y: 2, z: 4, core: 2. Of those that a mesh axis runs over, the one named last changes fastest.
Arguments:
- tokens: bfloat16 [8192, 2048], P(('rep', 'fs')), may hold values from -6 to 6
- mix_gain: float32 [2048], replicated, may hold values from 0.1 to 1.9
- w_gate_b: bfloat16 [2048, 1024], P('fs', 'tp'), may hold values from -0.125 to 0.125
- w_gate_c: bfloat16 [2048, 1024], P('fs', 'tp'), may hold values from -0.125 to 0.125
- w_conv_in: bfloat16 [2048, 1024], P('fs', 'tp'), may hold values from -0.125 to 0.125
- conv_taps: float32 [3, 1024], P(None, 'tp'), may hold values from -3 to 3
- w_mix_out: bfloat16 [1024, 2048], P('tp', 'fs'), may hold values from -0.1875 to 0.1875
- ffn_gain: float32 [2048], replicated, may hold values from 0.1 to 1.9
- w_ffn_gate: bfloat16 [2048, 2816], P('fs', 'tp'), may hold values from -0.125 to 0.125
- w_ffn_up: bfloat16 [2048, 2816], P('fs', 'tp'), may hold values from -0.125 to 0.125
- w_ffn_down: bfloat16 [2816, 2048], P('tp', 'fs'), may hold values from -0.109375 to 0.109375
Outputs:
- layer_out: bfloat16 [8192, 2048], P(('rep', 'fs', 'tp'))
All inputs are finite; a program needn't handle non-finite values.
Results may differ from a plain program's by a relative error of at most 0.014.
Values may be sent and summed in bfloat16 or wider, within the bound.
A program may use at most 64 MiB of HBM per device.

v0:
```python
import jax
import jax.numpy as jnp
from jax import lax
from jax.sharding import PartitionSpec as P

LEN = 128
EPSILON = 1e-06


def rms_scale(values, gain):
    return values * lax.rsqrt(jnp.mean(values * values, axis=-1, keepdims=True) + EPSILON) * gain


def causal_mix(product_in, conv_taps):
    shaped = product_in.reshape(product_in.shape[0] // LEN, LEN, product_in.shape[1])
    padded = jnp.pad(shaped, ((0, 0), (2, 0), (0, 0)))
    convolved = (
        conv_taps[0] * padded[:, :-2]
        + conv_taps[1] * padded[:, 1:-1]
        + conv_taps[2] * padded[:, 2:]
    )
    return convolved.reshape(product_in.shape)


def local(
    tokens,
    mix_gain,
    w_gate_b,
    w_gate_c,
    w_conv_in,
    conv_taps,
    w_mix_out,
    ffn_gain,
    w_ffn_gate,
    w_ffn_up,
    w_ffn_down,
):
    normed = rms_scale(tokens.astype(jnp.float32), mix_gain).astype(jnp.bfloat16)
    shard_rows = (
        lax.all_gather(w_gate_b, "fs", axis=0, tiled=True),
        lax.all_gather(w_gate_c, "fs", axis=0, tiled=True),
        lax.all_gather(w_conv_in, "fs", axis=0, tiled=True),
    )
    gate_b, gate_c, conv_in = tuple(
        (jnp.dot(normed, weight, preferred_element_type=jnp.float32) for weight in shard_rows)
    )
    gated = (gate_b * causal_mix(gate_c * conv_in, conv_taps)).astype(jnp.bfloat16)
    mix_columns = lax.all_gather(w_mix_out, "fs", axis=1, tiled=True)
    row_count = normed.shape[0] // lax.axis_size("tp")
    branch = lax.psum_scatter(
        jnp.dot(gated, mix_columns, preferred_element_type=jnp.float32).astype(jnp.bfloat16),
        "tp",
        scatter_dimension=0,
        tiled=True,
    ).astype(jnp.float32)
    own_rows = lax.dynamic_slice_in_dim(tokens, lax.axis_index("tp") * row_count, row_count, 0)
    stream = own_rows.astype(jnp.float32) + branch
    normed_two = rms_scale(stream, ffn_gain).astype(jnp.bfloat16)
    gate_rows, up_rows = (
        lax.all_gather(w_ffn_gate, "fs", axis=0, tiled=True),
        lax.all_gather(w_ffn_up, "fs", axis=0, tiled=True),
    )
    shard_rows = lax.all_gather(normed_two, "tp", axis=0, tiled=True)
    gate_part = jnp.dot(shard_rows, gate_rows, preferred_element_type=jnp.float32)
    up_part = jnp.dot(shard_rows, up_rows, preferred_element_type=jnp.float32)
    hidden = (jax.nn.silu(gate_part) * up_part).astype(jnp.bfloat16)
    down_columns = lax.all_gather(w_ffn_down, "fs", axis=1, tiled=True)
    ffn_branch = lax.psum_scatter(
        jnp.dot(hidden, down_columns, preferred_element_type=jnp.float32).astype(jnp.bfloat16),
        "tp",
        scatter_dimension=0,
        tiled=True,
    ).astype(jnp.float32)
    return (stream + ffn_branch).astype(jnp.bfloat16)


def solution(mesh):
    in_specs = (
        P(("rep", "fs"), None),
        P(),
        P("fs", "tp"),
        P("fs", "tp"),
        P("fs", "tp"),
        P(None, "tp"),
        P("tp", "fs"),
        P(),
        P("fs", "tp"),
        P("fs", "tp"),
        P("tp", "fs"),
    )
    out_specs = P(("rep", "fs", "tp"), None)
    return jax.shard_map(local, mesh=mesh, in_specs=in_specs, out_specs=out_specs, check_vma=False)
```

profile of v0, /device:TPU:0, one launch (start us, length us, event | category | flops | bytes accessed | tf_op | source)
XLA Modules:
  0.0 424.1 jit_solution(1093069393383213584)
XLA Ops:
  6.5 0.7 all-gather.11.cloned.1.call-update
  7.3 0.7 all-gather.13.cloned.1.call-update
  8.1 0.7 all-gather.15.cloned.1.call-update
  9.9 37.2 %all-gather.11.cloned.1.call-done = bf16[2048,512]{1,0:T(8,128)(2,1)} async-done(((bf16[512,512]{1,0:T(8,128)(2,1)}), bf16[2048,512]{1,0:T(8,128)(2,1)}) %all-gather.11.cloned.1.call-update) | async-done | bytes 2097168 | tf_op jit(solution)/shard_map/all_gather | solution.py:41
  47.1 2.9 fusion.11
  50.0 34.2 %all-gather.13.cloned.1.call-done = bf16[2048,512]{1,0:T(8,128)(2,1)} async-done(((bf16[512,512]{1,0:T(8,128)(2,1)}), bf16[2048,512]{1,0:T(8,128)(2,1)}) %all-gather.13.cloned.1.call-update) | async-done | bytes 2097168 | tf_op jit(solution)/shard_map/all_gather | solution.py:42
  84.2 2.9 convolution_multiply_fusion.1
  87.4 33.7 %all-gather.15.cloned.1.call-done = bf16[512,2048]{1,0:T(8,128)(2,1)} async-done(((bf16[512,512]{1,0:T(8,128)(2,1)}), bf16[512,2048]{1,0:T(8,128)(2,1)}) %all-gather.15.cloned.1.call-update) | async-done | bytes 2097168 | tf_op jit(solution)/shard_map/all_gather | solution.py:48
  121.1 36.9 %all-gather.9.cloned.1.call-done = bf16[2048,512]{1,0:T(8,128)(2,1)} async-done(((bf16[512,512]{1,0:T(8,128)(2,1)}), bf16[2048,512]{1,0:T(8,128)(2,1)}) %all-gather.9.cloned.1.call-update) | async-done | bytes 2097168 | tf_op jit(solution)/shard_map/all_gather | solution.py:40
  158.0 5.9 %convolution_convert_fusion = bf16[512,2048]{1,0:T(8,128)(2,1)} fusion(bf16[512,2048]{1,0:T(8,128)(2,1)} %all-gather.15.cloned.1.call-done, f32[512,512]{1,0:T(8,128)S(1)} %bitcast.14, bf16[2048,512]{1,0:T(8,128)(2,1)} %all-gather.9.cloned.1.call-done, bf16[512,2048]{1,0:T(8,128)(2,1)S(1)} %copy-done, f32[2048]{0:T(1024)S(1)} %copy-done.4, ...), kind=kOutput, calls=%fused_computation.7 | convolution fusion | flops 2153250816 | bytes 9447424 | tf_op jit(solution)/shard_map/dot_general | solution.py:51
  164.0 0.5 all-gather.19.cloned.1.call-update
  164.6 9.3 %reduce-scatter.3.cloned.1.call-done = bf16[256,2048]{1,0:T(8,128)(2,1)} async-done(((bf16[512,2048]{1,0:T(8,128)(2,1)}), bf16[256,2048]{1,0:T(8,128)(2,1)}) %reduce-scatter.3.cloned.1.call-update) | async-done | bytes 1048592 | tf_op jit(solution)/shard_map/reduce_scatter | solution.py:50
  173.9 1.7 multiply_reduce_fusion
  175.6 1.5 multiply_convert_fusion
  177.2 0.7 all-gather.21.cloned.1.call-update
  177.9 0.7 all-gather.23.cloned.1.call-update
  178.8 63.7 %all-gather.19.cloned.1.call-done = bf16[2048,1408]{1,0:T(8,128)(2,1)} async-done(((bf16[512,1408]{1,0:T(8,128)(2,1)}), bf16[2048,1408]{1,0:T(8,128)(2,1)}) %all-gather.19.cloned.1.call-update) | async-done | bytes 5767184 | tf_op jit(solution)/shard_map/all_gather | solution.py:60
  242.5 12.1 %all-gather.17.cloned.1.call-done = bf16[512,2048]{1,0:T(8,128)(2,1)} async-done(((bf16[256,2048]{1,0:T(8,128)(2,1)}), bf16[512,2048]{1,0:T(8,128)(2,1)}) %all-gather.17.cloned.1.call-update) | async-done | bytes 2097168 | tf_op jit(solution)/shard_map/all_gather | solution.py:63
  254.7 8.2 %fusion.16 = f32[512,1408]{1,0:T(8,128)} fusion(bf16[512,2048]{1,0:T(8,128)(2,1)} %all-gather.17.cloned.1.call-done, bf16[2048,1408]{1,0:T(8,128)(2,1)} %all-gather.19.cloned.1.call-done), kind=kOutput, calls=%fused_computation.27 | convolution fusion | flops 2952790016 | bytes 10747904 | tf_op jit(solution)/shard_map/dot_general | solution.py:64
  262.9 60.5 %all-gather.21.cloned.1.call-done = bf16[2048,1408]{1,0:T(8,128)(2,1)} async-done(((bf16[512,1408]{1,0:T(8,128)(2,1)}), bf16[2048,1408]{1,0:T(8,128)(2,1)}) %all-gather.21.cloned.1.call-update) | async-done | bytes 5767184 | tf_op jit(solution)/shard_map/all_gather | solution.py:61
  323.4 67.4 %all-gather.23.cloned.1.call-done = bf16[1408,2048]{1,0:T(8,128)(2,1)} async-done(((bf16[1408,512]{1,0:T(8,128)(2,1)}), bf16[1408,2048]{1,0:T(8,128)(2,1)}) %all-gather.23.cloned.1.call-update) | async-done | bytes 5767184 | tf_op jit(solution)/shard_map/all_gather | solution.py:67
  390.8 13.8 %convolution_convert_fusion.1 = bf16[512,2048]{1,0:T(8,128)(2,1)} fusion(bf16[1408,2048]{1,0:T(8,128)(2,1)} %all-gather.23.cloned.1.call-done, bf16[512,2048]{1,0:T(8,128)(2,1)} %all-gather.17.cloned.1.call-done, bf16[2048,1408]{1,0:T(8,128)(2,1)} %all-gather.21.cloned.1.call-done, f32[512,1408]{1,0:T(8,128)} %fusion.16), kind=kOutput, calls=%fused_computation.8 | convolution fusion | flops 5910953984 | bytes 18612224 | tf_op jit(solution)/shard_map/dot_general | solution.py:69
  404.6 9.9 %reduce-scatter.5.cloned.1.call-done = bf16[256,2048]{1,0:T(8,128)(2,1)} async-done(((bf16[512,2048]{1,0:T(8,128)(2,1)}), bf16[256,2048]{1,0:T(8,128)(2,1)}) %reduce-scatter.5.cloned.1.call-update) | async-done | bytes 1048592 | tf_op jit(solution)/shard_map/reduce_scatter | solution.py:68
  414.5 2.7 add_convert_fusion
  (29 shorter events, 1.9 us)
Async XLA Ops:
  6.5 2.8 copy-start
  6.5 40.6 %all-gather.11.cloned.1.call-start = ((), (), s32[]{:S(2)}) async-start(), calls=%async_computation.3 | async-start | bytes 2621440 | tf_op jit(solution)/shard_map/all_gather | solution.py:41
  6.5 3.3 copy-start.3
  6.5 40.6 %copy-start.4 = (f32[2048]{0:T(1024)S(1)}, f32[2048]{0:T(1024)}, u32[]{:S(2)}) copy-start(f32[2048]{0:T(1024)} %param.12) | copy-start | bytes 24580
  7.3 76.9 %all-gather.13.cloned.1.call-start = ((), (), s32[]{:S(2)}) async-start(), calls=%async_computation.4 | async-start | bytes 2621440 | tf_op jit(solution)/shard_map/all_gather | solution.py:42
  8.0 113.1 %all-gather.15.cloned.1.call-start = ((), (), s32[]{:S(2)}) async-start(), calls=%async_computation.5 | async-start | bytes 2621440 | tf_op jit(solution)/shard_map/all_gather | solution.py:48
  8.7 149.2 %all-gather.9.cloned.1.call-start = ((), (), s32[]{:S(2)}) async-start(), calls=%async_computation.2 | async-start | bytes 2621440 | tf_op jit(solution)/shard_map/all_gather | solution.py:40
  9.3 164.5 %reduce-scatter.3.cloned.1.call-start = ((), (), s32[]{:S(2)}) async-start(), calls=%async_computation.6 | async-start | bytes 3145728 | tf_op jit(solution)/shard_map/reduce_scatter | solution.py:50
  163.9 11.7 %copy-start.2 = (f32[2048]{0:T(1024)S(1)}, f32[2048]{0:T(1024)}, u32[]{:S(2)}) copy-start(f32[2048]{0:T(1024)} %param.18) | copy-start | bytes 24580
  164.0 78.6 %all-gather.19.cloned.1.call-start = ((), (), s32[]{:S(2)}) async-start(), calls=%async_computation.8 | async-start | bytes 7208960 | tf_op jit(solution)/shard_map/all_gather | solution.py:60
  164.5 90.2 %all-gather.17.cloned.1.call-start = ((), (), s32[]{:S(2)}) async-start(), calls=%async_computation.7 | async-start | bytes 3145728 | tf_op jit(solution)/shard_map/all_gather | solution.py:63
  173.9 1.8 copy-start.1
  177.1 146.3 %all-gather.21.cloned.1.call-start = ((), (), s32[]{:S(2)}) async-start(), calls=%async_computation.9 | async-start | bytes 7208960 | tf_op jit(solution)/shard_map/all_gather | solution.py:61
  177.9 212.9 %all-gather.23.cloned.1.call-start = ((), (), s32[]{:S(2)}) async-start(), calls=%async_computation.10 | async-start | bytes 7208960 | tf_op jit(solution)/shard_map/all_gather | solution.py:67
  178.6 235.9 %reduce-scatter.5.cloned.1.call-start = ((), (), s32[]{:S(2)}) async-start(), calls=%async_computation.11 | async-start | bytes 3145728 | tf_op jit(solution)/shard_map/reduce_scatter | solution.py:68
Sparse Core Ops, SparseCore 0:
  9.2 37.8 all-gather.10
  49.0 35.1 all-gather.12
  86.0 35.0 all-gather.14
  122.8 35.1 all-gather.8
  164.1 9.7 reduce-scatter.2
  175.6 66.9 all-gather.18
  244.1 10.5 all-gather.16
  256.5 66.8 all-gather.20
  325.2 65.5 all-gather.22
  404.8 9.7 reduce-scatter.4
where the time goes:
time: 424 us
  waiting for transfers between devices  369 us (87%)
  matrix products  33.8 us (8%)
  between operations  13.6 us (3%)
  other arithmetic  6.75 us (2%)
    all_gather x1, waiting for transfers between devices, local(): down_columns = lax.all_gather(w_ffn_down, 'fs', axis=1, tiled=True)  67.4 us
    all_gather x1, waiting for transfers between devices, local(): lax.all_gather(w_ffn_gate, 'fs', axis=0, tiled=True)  63.7 us
    all_gather x1, waiting for transfers between devices, local(): lax.all_gather(w_ffn_up, 'fs', axis=0, tiled=True)  60.5 us
    all_gather x1, waiting for transfers between devices, local(): lax.all_gather(w_gate_c, 'fs', axis=0, tiled=True)  37.2 us
    all_gather x1, waiting for transfers between devices, local(): lax.all_gather(w_gate_b, 'fs', axis=0, tiled=True)  36.9 us
    all_gather x1, waiting for transfers between devices, local(): lax.all_gather(w_conv_in, 'fs', axis=0, tiled=True)  34.2 us
    all_gather x1, waiting for transfers between devices, local(): mix_columns = lax.all_gather(w_mix_out, 'fs', axis=1, tiled=True)  33.7 us
    dot_general x1, matrix products, local(): jnp.dot(hidden, down_columns, preferred_element_type=jnp.float32)  13.8 us
  transfers between devices with their start and end apart: 10, of which 10 were waited for; matrix products, arithmetic and copies ran while one was open for 4% of the time, Pallas kernels for 0%

commit v1 on v0

--- a/solution.py
+++ b/solution.py
@@ -64,7 +64,25 @@
     gate_part = jnp.dot(shard_rows, gate_rows, preferred_element_type=jnp.float32)
     up_part = jnp.dot(shard_rows, up_rows, preferred_element_type=jnp.float32)
     hidden = (jax.nn.silu(gate_part) * up_part).astype(jnp.bfloat16)
-    down_columns = lax.all_gather(w_ffn_down, "fs", axis=1, tiled=True)
+
+    def expand_the_sheet(local_block, axis_tag="fs"):
+        width = jax.lax.axis_size(axis_tag)
+        kept_rows = []
+        for to_i in range(1, width):
+            kept_rows.append((to_i - 1, to_i))
+        r_now = kept_rows + [(width - 1, 0)]
+        plain = local_block
+        pages = [plain]
+        for _ in range(width - 1):
+            plain = jax.lax.ppermute(plain, axis_tag, r_now)
+            pages += [plain]
+        return jnp.roll(
+            jnp.concatenate([*reversed(pages)], 1),
+            (jax.lax.axis_index(axis_tag) + 1) * plain.shape[1],
+            1,
+        )
+
+    down_columns = expand_the_sheet(w_ffn_down)
     ffn_branch = lax.psum_scatter(
         jnp.dot(hidden, down_columns, preferred_element_type=jnp.float32).astype(jnp.bfloat16),
         "tp",

time: 424 us -> 412 us (0.972)
  waiting for transfers between devices: 369 us -> 335 us
  local copies, waits for them, and re-layouts: 0.03 us -> 17.6 us
  starting transfers between devices: 0.53 us -> 5.31 us
    ppermute x0 -> x3, waiting for transfers between devices: none -> 154 us  [expand_the_sheet(): plain = jax.lax.ppermute(plain, axis_tag, r_now)]
    all_gather x1 -> x0, waiting for transfers between devices: 67.4 us -> none  [local(): down_columns = lax.all_gather(w_ffn_down, 'fs', axis=1, tiled=True)]
    all_gather x1, waiting for transfers between devices: 63.7 us -> 0.01 us  [local(): lax.all_gather(w_ffn_gate, 'fs', axis=0, tiled=True)]
    all_gather x1, waiting for transfers between devices: 60.5 us -> 15.8 us  [local(): lax.all_gather(w_ffn_up, 'fs', axis=0, tiled=True)]
    unnamed x10 -> x23, local copies, waits for them, and re-layouts: 0.02 us -> 16.3 us
    all_gather x1, waiting for transfers between devices: 12.1 us -> 0.01 us  [local(): shard_rows = lax.all_gather(normed_two, 'tp', axis=0, tiled=True)]
    ppermute x0 -> x3, starting transfers between devices: none -> 4.99 us  [expand_the_sheet(): plain = jax.lax.ppermute(plain, axis_tag, r_now)]
  transfers between devices with their start and end apart: 10 -> 12, of which waited for: 10 -> 10; matrix products, arithmetic and copies ran while one was open for 4% -> 8% of each run, Pallas kernels for 0% -> 0%
where the time goes in v1:
time: 412 us
  waiting for transfers between devices  335 us (81%)
  matrix products  34.1 us (8%)
  local copies, waits for them, and re-layouts  17.6 us (4%)
  between operations  13.3 us (3%)
  other arithmetic  6.75 us (2%)
  starting transfers between devices  5.31 us (1%)
    ppermute x3, waiting for transfers between devices, expand_the_sheet(): plain = jax.lax.ppermute(plain, axis_tag, r_now)  154 us
    all_gather x1, waiting for transfers between devices, local(): lax.all_gather(w_gate_c, 'fs', axis=0, tiled=True)  37.2 us
    all_gather x1, waiting for transfers between devices, local(): lax.all_gather(w_gate_b, 'fs', axis=0, tiled=True)  36.9 us
    all_gather x1, waiting for transfers between devices, local(): lax.all_gather(w_conv_in, 'fs', axis=0, tiled=True)  34.2 us
    all_gather x1, waiting for transfers between devices, local(): mix_columns = lax.all_gather(w_mix_out, 'fs', axis=1, tiled=True)  33.7 us
    unnamed x23, local copies, waits for them, and re-layouts  16.3 us
    all_gather x1, waiting for transfers between devices, local(): lax.all_gather(w_ffn_up, 'fs', axis=0, tiled=True)  15.8 us
    dot_general x1, matrix products, local(): jnp.dot(hidden, down_columns, preferred_element_type=jnp.float32)  14 us
  transfers between devices with their start and end apart: 12, of which 10 were waited for; matrix products, arithmetic and copies ran while one was open for 8% of the time, Pallas kernels for 0%

profile of v1, /device:TPU:0, one launch (start us, length us, event | category | flops | bytes accessed | tf_op | source)
XLA Modules:
  0.0 411.6 jit_solution(6324177853650509527)
XLA Ops:
  9.9 37.2 %all-gather.10.cloned.1.call-done = bf16[2048,512]{1,0:T(8,128)(2,1)} async-done(((bf16[512,512]{1,0:T(8,128)(2,1)}), bf16[2048,512]{1,0:T(8,128)(2,1)}) %all-gather.10.cloned.1.call-update) | async-done | bytes 2097168 | tf_op jit(solution)/shard_map/all_gather | solution.py:41
  47.1 2.9 fusion.17
  50.0 34.2 %all-gather.12.cloned.1.call-done = bf16[2048,512]{1,0:T(8,128)(2,1)} async-done(((bf16[512,512]{1,0:T(8,128)(2,1)}), bf16[2048,512]{1,0:T(8,128)(2,1)}) %all-gather.12.cloned.1.call-update) | async-done | bytes 2097168 | tf_op jit(solution)/shard_map/all_gather | solution.py:42
  84.2 2.9 convolution_multiply_fusion.1
  87.4 33.7 %all-gather.14.cloned.1.call-done = bf16[512,2048]{1,0:T(8,128)(2,1)} async-done(((bf16[512,512]{1,0:T(8,128)(2,1)}), bf16[512,2048]{1,0:T(8,128)(2,1)}) %all-gather.14.cloned.1.call-update) | async-done | bytes 2097168 | tf_op jit(solution)/shard_map/all_gather | solution.py:48
  121.1 36.9 %all-gather.8.cloned.1.call-done = bf16[2048,512]{1,0:T(8,128)(2,1)} async-done(((bf16[512,512]{1,0:T(8,128)(2,1)}), bf16[2048,512]{1,0:T(8,128)(2,1)}) %all-gather.8.cloned.1.call-update) | async-done | bytes 2097168 | tf_op jit(solution)/shard_map/all_gather | solution.py:40
  158.0 6.0 %convolution_convert_fusion = bf16[512,2048]{1,0:T(8,128)(2,1)} fusion(bf16[512,2048]{1,0:T(8,128)(2,1)} %all-gather.14.cloned.1.call-done, f32[512,512]{1,0:T(8,128)S(1)} %bitcast.13, bf16[2048,512]{1,0:T(8,128)(2,1)} %all-gather.8.cloned.1.call-done, bf16[512,2048]{1,0:T(8,128)(2,1)S(1)} %copy-done, f32[2048]{0:T(1024)S(1)} %copy-done.7, ...), kind=kOutput, calls=%fused_computation.10 | convolution fusion | flops 2153250816 | bytes 9447424 | tf_op jit(solution)/shard_map/dot_general | solution.py:51
  164.6 9.2 %reduce-scatter.3.cloned.1.call-done = bf16[256,2048]{1,0:T(8,128)(2,1)} async-done(((bf16[512,2048]{1,0:T(8,128)(2,1)}), bf16[256,2048]{1,0:T(8,128)(2,1)}) %reduce-scatter.3.cloned.1.call-update) | async-done | bytes 1048592 | tf_op jit(solution)/shard_map/reduce_scatter | solution.py:50
  173.9 1.7 multiply_reduce_fusion
  175.6 1.5 multiply_convert_fusion
  177.9 1.9 collective-permute-start
  179.8 50.1 %collective-permute-done = bf16[1408,512]{1,0:T(8,128)(2,1)S(1)} collective-permute-done((bf16[1408,512]{1,0:T(8,128)(2,1)}, bf16[1408,512]{1,0:T(8,128)(2,1)S(1)}, u32[]{:S(2)}, u32[]{:S(2)}) %collective-permute-start) | collective-permute-done | bytes 1441824 | tf_op jit(solution)/shard_map/ppermute | solution.py:77
  231.1 2.3 collective-permute-start.1
  233.5 56.8 %collective-permute-done.1 = bf16[1408,512]{1,0:T(8,128)(2,1)} collective-permute-done((bf16[1408,512]{1,0:T(8,128)(2,1)S(1)}, bf16[1408,512]{1,0:T(8,128)(2,1)}, u32[]{:S(2)}, u32[]{:S(2)}) %collective-permute-start.1) | collective-permute-done | bytes 1441824 | tf_op jit(solution)/shard_map/ppermute | solution.py:77
  291.0 46.8 %collective-permute-done.2 = bf16[1408,512]{1,0:T(8,128)(2,1)} collective-permute-done((bf16[1408,512]{1,0:T(8,128)(2,1)}, bf16[1408,512]{1,0:T(8,128)(2,1)}, u32[]{:S(2)}, u32[]{:S(2)}) %collective-permute-start.2) | collective-permute-done | bytes 1441824 | tf_op jit(solution)/shard_map/ppermute | solution.py:77
  337.8 2.7 constant_dynamic-update-slice_fusion.7
  340.5 2.8 constant_dynamic-update-slice_fusion.6
  346.4 2.7 constant_dynamic-update-slice_fusion.3
  349.0 2.6 constant_dynamic-update-slice_fusion.2
  354.3 8.3 %fusion.22 = f32[512,1408]{1,0:T(8,128)} fusion(bf16[512,2048]{1,0:T(8,128)(2,1)} %all-gather.16.cloned.1.call-done, bf16[2048,1408]{1,0:T(8,128)(2,1)} %all-gather.18.cloned.1.call-done), kind=kOutput, calls=%fused_computation.38 | convolution fusion | flops 2952790016 | bytes 10747904 | tf_op jit(solution)/shard_map/dot_general | solution.py:64
  362.6 15.8 %all-gather.20.cloned.1.call-done = bf16[2048,1408]{1,0:T(8,128)(2,1)} async-done(((bf16[512,1408]{1,0:T(8,128)(2,1)}), bf16[2048,1408]{1,0:T(8,128)(2,1)}) %all-gather.20.cloned.1.call-update) | async-done | bytes 5767184 | tf_op jit(solution)/shard_map/all_gather | solution.py:61
  378.4 14.0 %fusion.6 = bf16[512,2048]{1,0:T(8,128)(2,1)} fusion(bf16[1408,4096]{1,0:T(8,128)(2,1)} %constant_dynamic-update-slice_fusion, s32[]{:T(128)S(6)} %select_n.18, bf16[512,2048]{1,0:T(8,128)(2,1)} %all-gather.16.cloned.1.call-done, bf16[2048,1408]{1,0:T(8,128)(2,1)} %all-gather.20.cloned.1.call-done, f32[512,1408]{1,0:T(8,128)} %fusion.22), kind=kOutput, calls=%fused_computation.9 | convolution fusion | flops 5910953984 | bytes 18612228 | tf_op jit(solution)/shard_map/dot_general | solution.py:87
  392.4 9.9 %reduce-scatter.5.cloned.1.call-done = bf16[256,2048]{1,0:T(8,128)(2,1)} async-done(((bf16[512,2048]{1,0:T(8,128)(2,1)}), bf16[256,2048]{1,0:T(8,128)(2,1)}) %reduce-scatter.5.cloned.1.call-update) | async-done | bytes 1048592 | tf_op jit(solution)/shard_map/reduce_scatter | solution.py:86
  402.4 2.7 add_convert_fusion
  (46 shorter events, 12.7 us)
Async XLA Ops:
  6.5 2.8 copy-start
  6.5 3.3 copy-start.6
  6.5 40.6 %copy-start.7 = (f32[2048]{0:T(1024)S(1)}, f32[2048]{0:T(1024)}, u32[]{:S(2)}) copy-start(f32[2048]{0:T(1024)} %param.12) | copy-start | bytes 24580
  6.5 40.6 %all-gather.10.cloned.1.call-start = ((), (), s32[]{:S(2)}) async-start(), calls=%async_computation.3 | async-start | bytes 2621440 | tf_op jit(solution)/shard_map/all_gather | solution.py:41
  7.3 76.9 %all-gather.12.cloned.1.call-start = ((), (), s32[]{:S(2)}) async-start(), calls=%async_computation.4 | async-start | bytes 2621440 | tf_op jit(solution)/shard_map/all_gather | solution.py:42
  8.0 113.1 %all-gather.14.cloned.1.call-start = ((), (), s32[]{:S(2)}) async-start(), calls=%async_computation.5 | async-start | bytes 2621440 | tf_op jit(solution)/shard_map/all_gather | solution.py:48
  8.7 149.2 %all-gather.8.cloned.1.call-start = ((), (), s32[]{:S(2)}) async-start(), calls=%async_computation.2 | async-start | bytes 2621440 | tf_op jit(solution)/shard_map/all_gather | solution.py:40
  9.3 164.6 %reduce-scatter.3.cloned.1.call-start = ((), (), s32[]{:S(2)}) async-start(), calls=%async_computation.6 | async-start | bytes 3145728 | tf_op jit(solution)/shard_map/reduce_scatter | solution.py:50
  164.0 11.6 %copy-start.5 = (f32[2048]{0:T(1024)S(1)}, f32[2048]{0:T(1024)}, u32[]{:S(2)}) copy-start(f32[2048]{0:T(1024)} %param.18) | copy-start | bytes 24580
  164.0 190.2 %all-gather.18.cloned.1.call-start = ((), (), s32[]{:S(2)}) async-start(), calls=%async_computation.8 | async-start | bytes 7208960 | tf_op jit(solution)/shard_map/all_gather | solution.py:60
  164.6 189.7 %all-gather.16.cloned.1.call-start = ((), (), s32[]{:S(2)}) async-start(), calls=%async_computation.7 | async-start | bytes 3145728 | tf_op jit(solution)/shard_map/all_gather | solution.py:63
  173.9 1.8 copy-start.1
  177.1 201.3 %all-gather.20.cloned.1.call-start = ((), (), s32[]{:S(2)}) async-start(), calls=%async_computation.9 | async-start | bytes 7208960 | tf_op jit(solution)/shard_map/all_gather | solution.py:61
  177.9 224.5 %reduce-scatter.5.cloned.1.call-start = ((), (), s32[]{:S(2)}) async-start(), calls=%async_computation.10 | async-start | bytes 3145728 | tf_op jit(solution)/shard_map/reduce_scatter | solution.py:86
  177.9 52.0 %collective-permute-start = (bf16[1408,512]{1,0:T(8,128)(2,1)}, bf16[1408,512]{1,0:T(8,128)(2,1)S(1)}, u32[]{:S(2)}, u32[]{:S(2)}) collective-permute-start(bf16[1408,512]{1,0:T(8,128)(2,1)} %param.21), channel_id=1, source_target_pairs={{0,2},{2,4},{4,6},{6,0},{1,3},{3,5},{5,7},{7,1},{8,10},{10,12},{12... | collective-permute-start | bytes 4325384 | tf_op jit(solution)/shard_map/ppermute | solution.py:77
  230.0 1.2 copy-start.3
  231.1 59.1 %collective-permute-start.1 = (bf16[1408,512]{1,0:T(8,128)(2,1)S(1)}, bf16[1408,512]{1,0:T(8,128)(2,1)}, u32[]{:S(2)}, u32[]{:S(2)}) collective-permute-start(bf16[1408,512]{1,0:T(8,128)(2,1)S(1)} %collective-permute-done), channel_id=1, source_target_pairs={{0,2},{2,4},{4,6},{6,0},{1,3},{3,5},{5,7},{7,1},{8,10},{10,12},{12... | collective-permute-start | bytes 4325384 | tf_op jit(solution)/shard_map/ppermute | solution.py:77
  290.3 47.6 %collective-permute-start.2 = (bf16[1408,512]{1,0:T(8,128)(2,1)}, bf16[1408,512]{1,0:T(8,128)(2,1)}, u32[]{:S(2)}, u32[]{:S(2)}) collective-permute-start(bf16[1408,512]{1,0:T(8,128)(2,1)} %collective-permute-done.1), channel_id=1, source_target_pairs={{0,2},{2,4},{4,6},{6,0},{1,3},{3,5},{5,7},{7,1},{8,10},{10,12},{12... | collective-permute-start | bytes 4325384 | tf_op jit(solution)/shard_map/ppermute | solution.py:77
  340.5 2.8 copy-start.4
  343.2 1.9 copy-start.2
Sparse Core Ops, SparseCore 0:
  9.2 37.8 all-gather.9
  49.0 35.1 all-gather.11
  86.0 35.0 all-gather.13
  122.8 35.1 all-gather.7
  164.1 9.7 reduce-scatter.2
  175.6 109.3 all-gather.17
  286.6 10.6 all-gather.15
  299.1 79.2 all-gather.19
  392.6 9.7 reduce-scatter.4
